TPU v7x, 32 devices: a whole 2x2x4 slice. The times are simulated.
32 devices in a mesh: grp: 2 (over y), sp: 4 (over z), tp: 4 (over x, core).
Axes of the slice: x: 2, y: 2, z: 4, core: 2. Of those that a mesh axis runs over, the one named last changes fastest.
Arguments:
- query_first: bfloat16 [1536, 512], P(('grp', 'sp'), 'tp'), parts along dimension 0, may hold values from -172 to 172
- key_first: bfloat16 [1536, 512], P(('grp', 'sp'), 'tp'), parts along dimension 0, may hold values from -7.8 to 7.8
- query_second: bfloat16 [1536, 1024], P(('grp', 'sp'), 'tp'), parts along dimension 0, may hold values from -172 to 172
- key_second: bfloat16 [1536, 1024], P(('grp', 'sp'), 'tp'), parts along dimension 0, may hold values from -7.8 to 7.8
- values: bfloat16 [1536, 2, 512], P(('grp', 'sp'), None, 'tp'), parts along dimension 0, may hold values from -6 to 6
- lambdas: float32 [2, 4], P(None, 'tp'), may hold values from 0.3 to 0.8
- residual: bfloat16 [1536, 2048], P(('grp', 'sp'), 'tp'), parts along dimension 0, may hold values from -130 to 130
- norm_gain: bfloat16 [2048], P('tp'), may hold values from 0.099609375 to 1.8984375
- out_weight: bfloat16 [2, 512, 2048], P(None, 'tp'), may hold values from -0.1875 to 0.1875
- gate_weight: bfloat16 [2048, 5632], P('sp', 'tp'), may hold values from -0.125 to 0.125
- up_weight: bfloat16 [2048, 5632], P('sp', 'tp'), may hold values from -0.125 to 0.125
- down_weight: bfloat16 [5632, 2048], P('tp', 'sp'), may hold values from -0.078125 to 0.078125
Outputs:
- layer_out: bfloat16 [1536, 2048], P(('grp', 'sp'), 'tp'), parts along dimension 0
There are 2 independent parts, one for each index of `grp`. A program takes and returns all parts, laid end to end along the dimension named above; an argument that names none is the same for every part. Nothing has to cross between parts.
All inputs are finite; a program needn't handle non-finite values.
Results may differ from a plain program's by a relative error of at most 0.0065.
Values may be sent and summed in bfloat16 or wider, within the bound.
A program may use at most 128 MiB of HBM per device.

v0:
```python
import jax
import jax.numpy as jnp
from jax import lax
from jax.sharding import PartitionSpec as P

D = 2048


def per_device(
    query_first,
    key_first,
    query_second,
    key_second,
    values,
    lambdas,
    residual,
    norm_gain,
    out_weight,
    gate_weight,
    up_weight,
    down_weight,
):
    tok_rows = query_first.shape[0]
    heads_here = lambdas.shape[1]
    width_first = query_first.shape[1] // (2 * heads_here)
    width_second = query_second.shape[1] // (2 * heads_here)
    value_size = values.shape[2] // heads_here
    offset = lax.axis_index("sp") * tok_rows
    query_pos = offset + lax.broadcasted_iota(jnp.int32, (tok_rows, 1), 0)
    query_groups = (
        query_first.reshape(tok_rows, heads_here, 2, width_first),
        query_second.reshape(tok_rows, heads_here, 2, width_second),
    )
    key_widths = (width_first, width_second)
    start_state = (
        jnp.full((heads_here, 2, tok_rows, 1), -1e30, jnp.float32),
        jnp.zeros((heads_here, 2, tok_rows, 1), jnp.float32),
        jnp.zeros((heads_here, 2, tok_rows, value_size), jnp.float32),
    )
    states = (start_state, start_state)
    pieces = (
        lax.all_gather(key_first, "sp", axis=0, tiled=True),
        lax.all_gather(key_second, "sp", axis=0, tiled=True),
        lax.all_gather(values, "sp", axis=0, tiled=True),
    )
    piece_rows = pieces[0].shape[0]
    key_pos = lax.broadcasted_iota(jnp.int32, (1, piece_rows), 1)
    allowed = key_pos <= query_pos
    value_rows = pieces[2].reshape(piece_rows, 2, heads_here, value_size)
    results = []
    for group_idx in range(2):
        key_width = key_widths[group_idx]
        key_part = pieces[group_idx].reshape(piece_rows, heads_here, 2, key_width)
        scores = jnp.einsum(
            "qhmd,khmd->hmqk", query_groups[group_idx], key_part, preferred_element_type=jnp.float32
        ) * key_width ** (-0.5)
        scores = jnp.where(allowed, scores, -1e30)
        running, totals, weighted = states[group_idx]
        new_peak = jnp.maximum(running, jnp.max(scores, axis=-1, keepdims=True))
        weights = jnp.where(allowed, jnp.exp(scores - new_peak), 0.0)
        totals = jnp.sum(weights, axis=-1, keepdims=True)
        weighted = jnp.einsum(
            "hmqk,khe->hmqe",
            weights.astype(jnp.bfloat16),
            value_rows[:, group_idx],
            preferred_element_type=jnp.float32,
        )
        results.append((new_peak, totals, weighted))
    states = (results[0], results[1])
    map_out = jnp.stack([states[0][2] / states[0][1], states[1][2] / states[1][1]])
    differ = map_out[:, :, 0] - lambdas[:, :, None, None] * map_out[:, :, 1]
    head_scale = lax.rsqrt(jnp.mean(differ * differ, axis=-1, keepdims=True) + 1e-06)
    attended = (0.8 * differ * head_scale).astype(jnp.bfloat16)
    projection = out_weight.reshape(2, heads_here, value_size, out_weight.shape[2])
    mixed_part = jnp.einsum(
        "ghqe,gher->qr", attended, projection, preferred_element_type=jnp.float32
    )
    mixed = lax.psum_scatter(
        mixed_part.astype(jnp.bfloat16), "tp", scatter_dimension=1, tiled=True
    ).astype(jnp.float32)
    stream = residual.astype(jnp.float32) + mixed
    squares = lax.psum(jnp.sum(stream * stream, axis=1), "tp")
    row_scale = lax.rsqrt(squares[:, None] / D + 1e-06)
    normed = (stream * row_scale * norm_gain.astype(jnp.float32)).astype(jnp.bfloat16)
    full_rows = lax.all_gather(normed, "tp", axis=1, tiled=True)
    pieces = (
        lax.all_gather(gate_weight, "sp", axis=0, tiled=True),
        lax.all_gather(up_weight, "sp", axis=0, tiled=True),
    )
    gate = jnp.dot(full_rows, pieces[0], preferred_element_type=jnp.float32)
    up_part = jnp.dot(full_rows, pieces[1], preferred_element_type=jnp.float32)
    hidden = (jax.nn.silu(gate) * up_part).astype(jnp.bfloat16)
    partial_out = jnp.dot(
        hidden,
        lax.all_gather(down_weight, "sp", axis=1, tiled=True),
        preferred_element_type=jnp.float32,
    )
    ffn = lax.psum_scatter(
        partial_out.astype(jnp.bfloat16), "tp", scatter_dimension=1, tiled=True
    ).astype(jnp.float32)
    return (stream + 0.5 * ffn).astype(jnp.bfloat16)


def solution(mesh):
    return jax.shard_map(
        per_device,
        mesh=mesh,
        in_specs=(
            P(("grp", "sp"), "tp"),
            P(("grp", "sp"), "tp"),
            P(("grp", "sp"), "tp"),
            P(("grp", "sp"), "tp"),
            P(("grp", "sp"), None, "tp"),
            P(None, "tp"),
            P(("grp", "sp"), "tp"),
            P("tp"),
            P(None, "tp", None),
            P("sp", "tp"),
            P("sp", "tp"),
            P("tp", "sp"),
        ),
        out_specs=P(("grp", "sp"), "tp"),
        check_vma=False,
    )
```

profile of v0, /device:TPU:0, one launch (start us, length us, event | category | flops | bytes accessed | tf_op | source)
XLA Modules:
  0.0 419.4 jit_solution(9682786560967322755)
XLA Ops:
  7.4 0.0 copy-start
  7.4 0.0 reduce-scatter.3.cloned.1.call-start
  7.4 0.1 iota_compare_fusion
  7.6 16.6 %all_gather.23 = bf16[768,256]{1,0:T(8,128)(2,1)S(1)} all-gather(bf16[192,256]{1,0:T(8,128)(2,1)} %param.15), channel_id=1, replica_groups=mesh['grp'=2,'sp'=4,'tp'=4] {'sp'}, dimensions={0}, use_global_device_ids=true | all-gather | bytes 491520 | tf_op jit(solution)/shard_map/all_gather | solution.py:43
  24.2 0.2 copy.28
  24.4 0.0 copy-done.6
  24.4 14.4 %all_gather.21 = bf16[768,128]{1,0:T(8,128)(2,1)S(1)} all-gather(bf16[192,128]{1,0:T(8,128)(2,1)S(1)} %copy-done.6), channel_id=1, replica_groups=mesh['grp'=2,'sp'=4,'tp'=4] {'sp'}, dimensions={0}, use_global_device_ids=true | all-gather | bytes 245760 | tf_op jit(solution)/shard_map/all_gather | solution.py:42
  38.8 0.1 copy.26
  38.9 0.0 copy-done.5
  38.9 0.1 copy.25
  39.0 0.0 copy-done.4
  39.1 14.8 %all_gather.22 = bf16[768,2,128]{2,0,1:T(8,128)(2,1)S(1)} all-gather(bf16[192,2,128]{2,0,1:T(8,128)(2,1)S(1)} %copy.27), channel_id=1, replica_groups=mesh['grp'=2,'sp'=4,'tp'=4] {'sp'}, dimensions={0}, use_global_device_ids=true | all-gather | bytes 491520 | tf_op jit(solution)/shard_map/all_gather | solution.py:44
  53.8 0.0 copy-done.3
  53.8 0.5 fusion.34
  54.3 0.5 fusion.35
  54.8 0.7 fusion.6
  55.5 0.4 fusion.5
  55.9 0.0 copy-start.7
  55.9 0.4 fusion.4
  56.4 0.2 copy-done.7
  56.6 0.2 fusion.21
  56.8 0.0 copy-done
  56.8 1.3 fusion
  58.2 0.0 reduce-scatter.3.cloned.1.call-update
  58.2 0.0 all-gather.4.cloned.1.call-start
  58.3 0.5 all-gather.4.cloned.1.call-update
  58.8 0.0 copy-start.8
  58.8 0.0 copy-start.1
  58.8 0.0 all-gather.6.cloned.1.call-start
  58.9 0.5 all-gather.6.cloned.1.call-update
  59.4 0.0 all-gather.8.cloned.1.call-start
  59.4 0.5 all-gather.8.cloned.1.call-update
  60.0 0.0 reduce-scatter.5.cloned.1.call-start
  60.0 0.0 copy-done.8
  60.0 22.8 %reduce-scatter.3.cloned.1.call-done = bf16[192,512]{1,0:T(8,128)(2,1)} async-done(((bf16[192,2048]{1,0:T(8,128)(2,1)}), bf16[192,512]{1,0:T(8,128)(2,1)}) %reduce-scatter.3.cloned.1.call-update) | async-done | bytes 196624 | tf_op jit(solution)/shard_map/reduce_scatter | solution.py:78
  82.8 1.1 multiply_reduce_fusion
  83.9 6.1 %psum.7 = f32[192]{0:T(256)S(1)} all-reduce(f32[192]{0:T(256)S(1)} %multiply_reduce_fusion), channel_id=1, replica_groups=mesh['grp'=2,'sp'=4,'tp'=4] {'tp'}, use_global_device_ids=true, to_apply=%region_7.8 | all-reduce | flops 192 | bytes 1536 | tf_op jit(solution)/shard_map/psum | solution.py:82
  90.0 1.0 multiply_convert_fusion
  91.0 8.4 %all_gather.24 = bf16[192,2048]{1,0:T(8,128)(2,1)S(1)} all-gather(bf16[192,512]{1,0:T(8,128)(2,1)S(1)} %multiply_convert_fusion), channel_id=1, replica_groups=mesh['grp'=2,'sp'=4,'tp'=4] {'tp'}, dimensions={1}, use_global_device_ids=true | all-gather | bytes 983040 | tf_op jit(solution)/shard_map/all_gather | solution.py:85
  99.4 68.7 %all-gather.4.cloned.1.call-done = bf16[2048,1408]{1,0:T(8,128)(2,1)} async-done(((bf16[512,1408]{1,0:T(8,128)(2,1)}), bf16[2048,1408]{1,0:T(8,128)(2,1)}) %all-gather.4.cloned.1.call-update) | async-done | bytes 5767184 | tf_op jit(solution)/shard_map/all_gather | solution.py:87
  168.1 4.0 fusion.36
  172.1 0.0 copy-start.2
  172.1 102.2 %all-gather.6.cloned.1.call-done = bf16[2048,1408]{1,0:T(8,128)(2,1)} async-done(((bf16[512,1408]{1,0:T(8,128)(2,1)}), bf16[2048,1408]{1,0:T(8,128)(2,1)}) %all-gather.6.cloned.1.call-update) | async-done | bytes 5767184 | tf_op jit(solution)/shard_map/all_gather | solution.py:88
  274.4 106.3 %all-gather.8.cloned.1.call-done = bf16[1408,2048]{1,0:T(8,128)(2,1)} async-done(((bf16[1408,512]{1,0:T(8,128)(2,1)}), bf16[1408,2048]{1,0:T(8,128)(2,1)}) %all-gather.8.cloned.1.call-update) | async-done | bytes 5767184 | tf_op jit(solution)/shard_map/all_gather | solution.py:95
  380.6 7.9 %convolution_convert_fusion = bf16[192,2048]{1,0:T(8,128)(2,1)} fusion(bf16[1408,2048]{1,0:T(8,128)(2,1)} %all-gather.8.cloned.1.call-done, bf16[192,2048]{1,0:T(8,128)(2,1)S(1)} %all_gather.24, bf16[2048,1408]{1,0:T(8,128)(2,1)} %all-gather.6.cloned.1.call-done, f32[192,1408]{1,0:T(8,128)S(1)} %fusion.36), kind=kOutput, calls=%fused_computation.4 | convolution fusion | flops 2216607744 | bytes 14188544 | tf_op jit(solution)/shard_map/dot_general | solution.py:93
  388.5 0.0 reduce-scatter.5.cloned.1.call-update
  388.5 21.6 %reduce-scatter.5.cloned.1.call-done = bf16[192,512]{1,0:T(8,128)(2,1)} async-done(((bf16[192,2048]{1,0:T(8,128)(2,1)}), bf16[192,512]{1,0:T(8,128)(2,1)}) %reduce-scatter.5.cloned.1.call-update) | async-done | bytes 196624 | tf_op jit(solution)/shard_map/reduce_scatter | solution.py:98
  410.2 1.7 add_convert_fusion
  (12 shorter events, 0.1 us)
Async XLA Ops:
  7.4 49.5 %copy-start = (bf16[2,128,2048]{2,1,0:T(8,128)(2,1)S(1)}, bf16[2,128,2048]{2,1,0:T(8,128)(2,1)}, u32[]{:S(2)}) copy-start(bf16[2,128,2048]{2,1,0:T(8,128)(2,1)} %param.20) | copy-start | bytes 3145732
  7.4 17.0 %copy-start.6 = (bf16[192,128]{1,0:T(8,128)(2,1)S(1)}, bf16[192,128]{1,0:T(8,128)(2,1)}, u32[]{:S(2)}) copy-start(bf16[192,128]{1,0:T(8,128)(2,1)} %param.13) | copy-start | bytes 147460
  7.4 31.5 %copy-start.5 = (bf16[192,128]{1,0:T(8,128)(2,1)S(1)}, bf16[192,128]{1,0:T(8,128)(2,1)}, u32[]{:S(2)}) copy-start(bf16[192,128]{1,0:T(8,128)(2,1)} %param.12) | copy-start | bytes 147460
  7.4 31.7 %copy-start.4 = (bf16[192,2,128]{2,1,0:T(2,128)(2,1)S(1)}, bf16[192,2,128]{2,1,0:T(2,128)(2,1)}, u32[]{:S(2)}) copy-start(bf16[192,2,128]{2,1,0:T(2,128)(2,1)} %param.16) | copy-start | bytes 294916
  7.4 75.4 %reduce-scatter.3.cloned.1.call-start = ((), (), s32[]{:S(2)}) async-start(), calls=%async_computation.2 | async-start | bytes 983040 | tf_op jit(solution)/shard_map/reduce_scatter | solution.py:78
  24.2 29.6 %copy-start.3 = (bf16[192,256]{1,0:T(8,128)(2,1)S(1)}, bf16[192,256]{1,0:T(8,128)(2,1)}, u32[]{:S(2)}) copy-start(bf16[192,256]{1,0:T(8,128)(2,1)} %param.14) | copy-start | bytes 294916
  55.9 0.7 copy-start.7
  58.2 109.9 %all-gather.4.cloned.1.call-start = ((), (), s32[]{:S(2)}) async-start(), calls=%async_computation.3 | async-start | bytes 7208960 | tf_op jit(solution)/shard_map/all_gather | solution.py:87
  58.8 1.2 copy-start.8
  58.8 24.0 %copy-start.1 = (bf16[192,512]{1,0:T(8,128)(2,1)S(1)}, bf16[192,512]{1,0:T(8,128)(2,1)}, u32[]{:S(2)}) copy-start(bf16[192,512]{1,0:T(8,128)(2,1)} %param.18) | copy-start | bytes 589828
  58.8 215.6 %all-gather.6.cloned.1.call-start = ((), (), s32[]{:S(2)}) async-start(), calls=%async_computation.4 | async-start | bytes 7208960 | tf_op jit(solution)/shard_map/all_gather | solution.py:88
  59.4 321.3 %all-gather.8.cloned.1.call-start = ((), (), s32[]{:S(2)}) async-start(), calls=%async_computation.5 | async-start | bytes 7208960 | tf_op jit(solution)/shard_map/all_gather | solution.py:95
  60.0 350.2 %reduce-scatter.5.cloned.1.call-start = ((), (), s32[]{:S(2)}) async-start(), calls=%async_computation.6 | async-start | bytes 983040 | tf_op jit(solution)/shard_map/reduce_scatter | solution.py:98
  172.1 238.0 %copy-start.2 = (bf16[192,512]{1,0:T(8,128)(2,1)S(1)}, bf16[192,512]{1,0:T(8,128)(2,1)}, u32[]{:S(2)}) copy-start(bf16[192,512]{1,0:T(8,128)(2,1)} %reduce-scatter.3.cloned.1.call-done) | copy-start | bytes 589828
Sparse Core Ops, SparseCore 0:
  58.3 24.4 reduce-scatter.2
  388.7 21.4 reduce-scatter.4
Sparse Core Ops, SparseCore 1:
  60.3 107.8 all-gather.3
  169.5 104.8 all-gather.5
  275.8 104.8 all-gather.7
where the time goes:
time: 420 us; the launch traced here: 419 us
  waiting for transfers between devices  323 us (77%)
  blocking collectives  60.2 us (14%)
  between operations  15.2 us (4%)
  matrix products  15.1 us (4%)
  other arithmetic  4.87 us (1%)
    all_gather x1, waiting for transfers between devices, per_device(): lax.all_gather(down_weight, 'sp', axis=1, tiled=True)  106 us
    all_gather x1, waiting for transfers between devices, per_device(): lax.all_gather(up_weight, 'sp', axis=0, tiled=True)  102 us
    all_gather x1, waiting for transfers between devices, per_device(): lax.all_gather(gate_weight, 'sp', axis=0, tiled=True)  68.7 us
    reduce_scatter x1, waiting for transfers between devices, per_device(): lax.psum_scatter(mixed_part.astype(jnp.bfloat16), 'tp', scatter_dimension...  22.8 us
    reduce_scatter x1, waiting for transfers between devices, per_device(): lax.psum_scatter(partial_out.astype(jnp.bfloat16), 'tp', scatter_dimensio...  21.6 us
    all_gather x1, blocking collectives, per_device(): lax.all_gather(key_second, 'sp', axis=0, tiled=True)  16.6 us
    all_gather x1, blocking collectives, per_device(): lax.all_gather(values, 'sp', axis=0, tiled=True)  14.8 us
    all_gather x1, blocking collectives, per_device(): lax.all_gather(key_first, 'sp', axis=0, tiled=True)  14.4 us
  transfers between devices with their start and end apart: 5, of which 5 were waited for; matrix products, arithmetic and copies ran while one was open for 1% of the time, Pallas kernels for 0%

commit v1 on v0

--- a/solution.py
+++ b/solution.py
@@ -1,9 +1,27 @@
+import functools
 import jax
 import jax.numpy as jnp
 from jax import lax
 from jax.sharding import PartitionSpec as P
 
 D = 2048
+
+
+def manage_the_targets(tile_in, dim_k):
+    full_n = jax.lax.axis_size("sp")
+    queue = [tile_in]
+    for pp in range(1, full_n):
+        raw_out = jax.lax.ppermute(
+            queue[pp - 1], "sp", [(it, (it - 1) % full_n) for it in range(full_n)]
+        )
+        queue.append(raw_out)
+    f_next = jnp.concatenate(queue, axis=dim_k)
+    piece_out = jax.lax.axis_index("sp")
+    small = jnp.roll(f_next, piece_out * tile_in.shape[dim_k], axis=dim_k)
+    return small
+
+
+search_the_rails = functools.partial(manage_the_targets, dim_k=1)
 
 
 def per_device(
@@ -90,11 +108,7 @@
     gate = jnp.dot(full_rows, pieces[0], preferred_element_type=jnp.float32)
     up_part = jnp.dot(full_rows, pieces[1], preferred_element_type=jnp.float32)
     hidden = (jax.nn.silu(gate) * up_part).astype(jnp.bfloat16)
-    partial_out = jnp.dot(
-        hidden,
-        lax.all_gather(down_weight, "sp", axis=1, tiled=True),
-        preferred_element_type=jnp.float32,
-    )
+    partial_out = jnp.dot(hidden, search_the_rails(down_weight), preferred_element_type=jnp.float32)
     ffn = lax.psum_scatter(
         partial_out.astype(jnp.bfloat16), "tp", scatter_dimension=1, tiled=True
     ).astype(jnp.float32)

time: 420 us -> 388 us (0.924)
  waiting for transfers between devices: 323 us -> 268 us
  local copies, waits for them, and re-layouts: 0.68 us -> 19.5 us
    ppermute x0 -> x3, waiting for transfers between devices: none -> 154 us  [manage_the_targets(): jax.lax.ppermute(queue[pp - 1], 'sp', [(it, (it - 1) % full_n) for it in...]
    all_gather x1 -> x0, waiting for transfers between devices: 106 us -> none  [per_device(): lax.all_gather(down_weight, 'sp', axis=1, tiled=True)]
    all_gather x1, waiting for transfers between devices: 68.7 us -> 0.01 us  [per_device(): lax.all_gather(gate_weight, 'sp', axis=0, tiled=True)]
    reduce_scatter x1, waiting for transfers between devices: 22.8 us -> 0.01 us  [per_device(): lax.psum_scatter(mixed_part.astype(jnp.bfloat16), 'tp', scatter_dimension...]
    unnamed x20 -> x29, local copies, waits for them, and re-layouts: 0.37 us -> 16.3 us
    all_gather x1, waiting for transfers between devices: 102 us -> 92 us  [per_device(): lax.all_gather(up_weight, 'sp', axis=0, tiled=True)]
  transfers between devices with their start and end apart: 5 -> 7, of which waited for: 5 -> 5; matrix products, arithmetic and copies ran while one was open for 1% -> 6% of each run, Pallas kernels for 0% -> 0%
where the time goes in v1:
time: 388 us; the launch traced here: 387 us
  waiting for transfers between devices  268 us (69%)
  blocking collectives  60.4 us (16%)
  local copies, waits for them, and re-layouts  19.5 us (5%)
  matrix products  15.3 us (4%)
  between operations  15 us (4%)
  other arithmetic  4.89 us (1%)
    ppermute x3, waiting for transfers between devices, manage_the_targets(): jax.lax.ppermute(queue[pp - 1], 'sp', [(it, (it - 1) % full_n) for it in...  154 us
    all_gather x1, waiting for transfers between devices, per_device(): lax.all_gather(up_weight, 'sp', axis=0, tiled=True)  92 us
    reduce_scatter x1, waiting for transfers between devices, per_device(): lax.psum_scatter(partial_out.astype(jnp.bfloat16), 'tp', scatter_dimensio...  21.6 us
    all_gather x1, blocking collectives, per_device(): lax.all_gather(key_second, 'sp', axis=0, tiled=True)  16.6 us
    unnamed x29, local copies, waits for them, and re-layouts  16.3 us
    all_gather x1, blocking collectives, per_device(): lax.all_gather(values, 'sp', axis=0, tiled=True)  14.8 us
    all_gather x1, blocking collectives, per_device(): lax.all_gather(key_first, 'sp', axis=0, tiled=True)  14.4 us
    all_gather x1, blocking collectives, per_device(): full_rows = lax.all_gather(normed, 'tp', axis=1, tiled=True)  8.6 us
  transfers between devices with their start and end apart: 7, of which 5 were waited for; matrix products, arithmetic and copies ran while one was open for 6% of the time, Pallas kernels for 0%

profile of v1, /device:TPU:0, one launch (start us, length us, event | category | flops | bytes accessed | tf_op | source)
XLA Modules:
  0.0 387.1 jit_solution(781363093430632308)
XLA Ops:
  7.4 0.0 reduce-scatter.3.cloned.1.call-start
  7.4 16.6 %all_gather.20 = bf16[768,256]{1,0:T(8,128)(2,1)S(1)} all-gather(bf16[192,256]{1,0:T(8,128)(2,1)} %param.15), channel_id=1, replica_groups=mesh['grp'=2,'sp'=4,'tp'=4] {'sp'}, dimensions={0}, use_global_device_ids=true | all-gather | bytes 491520 | tf_op jit(solution)/shard_map/all_gather | solution.py:61
  24.0 0.2 copy.28
  24.2 0.1 iota_compare_fusion
  24.4 0.1 copy.25
  24.5 14.4 %all_gather.18 = bf16[768,128]{1,0:T(8,128)(2,1)S(1)} all-gather(bf16[192,128]{1,0:T(8,128)(2,1)S(1)} %copy-done.7), channel_id=1, replica_groups=mesh['grp'=2,'sp'=4,'tp'=4] {'sp'}, dimensions={0}, use_global_device_ids=true | all-gather | bytes 245760 | tf_op jit(solution)/shard_map/all_gather | solution.py:60
  38.9 0.1 copy.26
  39.1 14.8 %all_gather.19 = bf16[768,2,128]{2,0,1:T(8,128)(2,1)S(1)} all-gather(bf16[192,2,128]{2,0,1:T(8,128)(2,1)S(1)} %copy.27), channel_id=1, replica_groups=mesh['grp'=2,'sp'=4,'tp'=4] {'sp'}, dimensions={0}, use_global_device_ids=true | all-gather | bytes 491520 | tf_op jit(solution)/shard_map/all_gather | solution.py:62
  53.9 0.5 fusion.40
  54.3 0.5 fusion.41
  54.8 0.7 fusion.11
  55.5 0.4 fusion.9
  56.0 0.0 copy-start.8
  56.0 0.4 fusion.10
  56.4 0.2 copy-done.8
  56.6 0.2 fusion.26
  56.9 1.3 fusion.2
  58.2 0.0 reduce-scatter.3.cloned.1.call-update
  58.2 0.0 copy-start.1
  58.2 0.0 copy-start.9
  58.3 0.0 all-gather.3.cloned.1.call-start
  58.3 0.5 all-gather.3.cloned.1.call-update
  58.8 0.0 all-gather.5.cloned.1.call-start
  58.9 0.5 all-gather.5.cloned.1.call-update
  59.4 0.0 reduce-scatter.5.cloned.1.call-start
  59.5 0.1 copy-done.1
  59.6 3.5 collective-permute-start
  63.1 75.4 %collective-permute-done = bf16[1408,512]{1,0:T(8,128)(2,1)} collective-permute-done((bf16[1408,512]{1,0:T(8,128)(2,1)S(1)}, bf16[1408,512]{1,0:T(8,128)(2,1)}, u32[]{:S(2)}, u32[]{:S(2)}) %collective-permute-start) | collective-permute-done | bytes 1441824 | tf_op jit(solution)/shard_map/ppermute | solution.py:14
  138.5 1.3 constant_dynamic-update-slice_fusion.7
  139.8 77.4 %collective-permute-done.1 = bf16[1408,512]{1,0:T(8,128)(2,1)} collective-permute-done((bf16[1408,512]{1,0:T(8,128)(2,1)}, bf16[1408,512]{1,0:T(8,128)(2,1)}, u32[]{:S(2)}, u32[]{:S(2)}) %collective-permute-start.1) | collective-permute-done | bytes 1441824 | tf_op jit(solution)/shard_map/ppermute | solution.py:14
  217.2 2.7 constant_dynamic-update-slice_fusion.6
  219.8 1.1 multiply_reduce_fusion
  220.9 6.1 %psum.7 = f32[192]{0:T(256)S(1)} all-reduce(f32[192]{0:T(256)S(1)} %multiply_reduce_fusion), channel_id=1, replica_groups=mesh['grp'=2,'sp'=4,'tp'=4] {'tp'}, use_global_device_ids=true, to_apply=%region_7.8 | all-reduce | flops 192 | bytes 1536 | tf_op jit(solution)/shard_map/psum | solution.py:100
  227.0 1.0 multiply_convert_fusion
  228.0 8.6 %all_gather.21 = bf16[192,2048]{1,0:T(8,128)(2,1)S(1)} all-gather(bf16[192,512]{1,0:T(8,128)(2,1)S(1)} %multiply_convert_fusion), channel_id=1, replica_groups=mesh['grp'=2,'sp'=4,'tp'=4] {'tp'}, dimensions={1}, use_global_device_ids=true | all-gather | bytes 983040 | tf_op jit(solution)/shard_map/all_gather | solution.py:103
  236.6 2.7 constant_dynamic-update-slice_fusion.5
  239.3 0.8 collective-permute-done.2
  240.1 2.6 constant_dynamic-update-slice_fusion.4
  242.7 1.2 constant_dynamic-update-slice_fusion.3
  244.0 2.6 constant_dynamic-update-slice_fusion.2
  246.6 2.7 constant_dynamic-update-slice_fusion.1
  249.3 2.9 constant_dynamic-update-slice_fusion
  252.1 4.3 %fusion.42 = f32[192,1408]{1,0:T(8,128)S(1)} fusion(bf16[192,2048]{1,0:T(8,128)(2,1)S(1)} %all_gather.21, bf16[2048,1408]{1,0:T(8,128)(2,1)} %all-gather.3.cloned.1.call-done), kind=kOutput, calls=%fused_computation.71 | convolution fusion | flops 1107296256 | bytes 7634944 | tf_op jit(solution)/shard_map/dot_general | solution.py:108
  256.4 92.0 %all-gather.5.cloned.1.call-done = bf16[2048,1408]{1,0:T(8,128)(2,1)} async-done(((bf16[512,1408]{1,0:T(8,128)(2,1)}), bf16[2048,1408]{1,0:T(8,128)(2,1)}) %all-gather.5.cloned.1.call-update) | async-done | bytes 5767184 | tf_op jit(solution)/shard_map/all_gather | solution.py:106
  348.4 7.9 %fusion.4 = bf16[192,2048]{1,0:T(8,128)(2,1)} fusion(bf16[1408,4096]{1,0:T(8,128)(2,1)} %constant_dynamic-update-slice_fusion, s32[]{:T(128)S(6)} %select_n.35, bf16[192,2048]{1,0:T(8,128)(2,1)S(1)} %all_gather.21, bf16[2048,1408]{1,0:T(8,128)(2,1)} %all-gather.5.cloned.1.call-done, f32[192,1408]{1,0:T(8,128)S(1)} %fusion.42), kind=kOutput, calls=%fused_computation.6 | convolution fusion | flops 2216607744 | bytes 14188548 | tf_op jit(solution)/shard_map/dot_general | solution.py:111
  356.3 0.0 reduce-scatter.5.cloned.1.call-update
  356.3 21.6 %reduce-scatter.5.cloned.1.call-done = bf16[192,512]{1,0:T(8,128)(2,1)} async-done(((bf16[192,2048]{1,0:T(8,128)(2,1)}), bf16[192,512]{1,0:T(8,128)(2,1)}) %reduce-scatter.5.cloned.1.call-update) | async-done | bytes 196624 | tf_op jit(solution)/shard_map/reduce_scatter | solution.py:112
  378.0 1.7 add_convert_fusion
  (25 shorter events, 0.1 us)
Async XLA Ops:
  7.4 49.5 %copy-start = (bf16[2,128,2048]{2,1,0:T(8,128)(2,1)S(1)}, bf16[2,128,2048]{2,1,0:T(8,128)(2,1)}, u32[]{:S(2)}) copy-start(bf16[2,128,2048]{2,1,0:T(8,128)(2,1)} %param.20) | copy-start | bytes 3145732
  7.4 17.0 %copy-start.6 = (bf16[192,128]{1,0:T(8,128)(2,1)S(1)}, bf16[192,128]{1,0:T(8,128)(2,1)}, u32[]{:S(2)}) copy-start(bf16[192,128]{1,0:T(8,128)(2,1)} %param.12) | copy-start | bytes 147460
  7.4 17.1 %copy-start.7 = (bf16[192,128]{1,0:T(8,128)(2,1)S(1)}, bf16[192,128]{1,0:T(8,128)(2,1)}, u32[]{:S(2)}) copy-start(bf16[192,128]{1,0:T(8,128)(2,1)} %param.13) | copy-start | bytes 147460
  7.4 31.7 %copy-start.5 = (bf16[192,2,128]{2,1,0:T(2,128)(2,1)S(1)}, bf16[192,2,128]{2,1,0:T(2,128)(2,1)}, u32[]{:S(2)}) copy-start(bf16[192,2,128]{2,1,0:T(2,128)(2,1)} %param.16) | copy-start | bytes 294916
  7.4 46.5 %copy-start.4 = (bf16[192,256]{1,0:T(8,128)(2,1)S(1)}, bf16[192,256]{1,0:T(8,128)(2,1)}, u32[]{:S(2)}) copy-start(bf16[192,256]{1,0:T(8,128)(2,1)} %param.14) | copy-start | bytes 294916
  7.4 212.5 %reduce-scatter.3.cloned.1.call-start = ((), (), s32[]{:S(2)}) async-start(), calls=%async_computation.2 | async-start | bytes 983040 | tf_op jit(solution)/shard_map/reduce_scatter | solution.py:96
  56.0 0.7 copy-start.8
  58.2 1.4 copy-start.1
  58.2 80.2 %copy-start.9 = (bf16[512]{0:T(512)(128)(2,1)S(1)}, bf16[512]{0:T(512)(128)(2,1)}, u32[]{:S(2)}) copy-start(bf16[512]{0:T(512)(128)(2,1)} %param.19) | copy-start | bytes 3076
  58.3 193.9 %all-gather.3.cloned.1.call-start = ((), (), s32[]{:S(2)}) async-start(), calls=%async_computation.3 | async-start | bytes 7208960 | tf_op jit(solution)/shard_map/all_gather | solution.py:105
  58.8 289.6 %all-gather.5.cloned.1.call-start = ((), (), s32[]{:S(2)}) async-start(), calls=%async_computation.4 | async-start | bytes 7208960 | tf_op jit(solution)/shard_map/all_gather | solution.py:106
  59.4 318.5 %reduce-scatter.5.cloned.1.call-start = ((), (), s32[]{:S(2)}) async-start(), calls=%async_computation.5 | async-start | bytes 983040 | tf_op jit(solution)/shard_map/reduce_scatter | solution.py:112
  59.6 78.9 %collective-permute-start = (bf16[1408,512]{1,0:T(8,128)(2,1)S(1)}, bf16[1408,512]{1,0:T(8,128)(2,1)}, u32[]{:S(2)}, u32[]{:S(2)}) collective-permute-start(bf16[1408,512]{1,0:T(8,128)(2,1)S(1)} %copy-done.1), channel_id=1, source_target_pairs={{0,12},{4,0},{8,4},{12,8},{1,13},{5,1},{9,5},{13,9},{2,14},{6,2},{... | collective-permute-start | bytes 4325384 | tf_op jit(solution)/shard_map/ppermute | solution.py:14
  138.5 78.7 %collective-permute-start.1 = (bf16[1408,512]{1,0:T(8,128)(2,1)}, bf16[1408,512]{1,0:T(8,128)(2,1)}, u32[]{:S(2)}, u32[]{:S(2)}) collective-permute-start(bf16[1408,512]{1,0:T(8,128)(2,1)} %collective-permute-done), channel_id=1, source_target_pairs={{0,12},{4,0},{8,4},{12,8},{1,13},{5,1},{9,5},{13,9},{2,14},{6,2},{... | collective-permute-start | bytes 4325384 | tf_op jit(solution)/shard_map/ppermute | solution.py:14
  139.8 80.0 %copy-start.2 = (bf16[192,512]{1,0:T(8,128)(2,1)S(1)}, bf16[192,512]{1,0:T(8,128)(2,1)}, u32[]{:S(2)}) copy-start(bf16[192,512]{1,0:T(8,128)(2,1)} %param.18) | copy-start | bytes 589828
  217.2 22.9 %collective-permute-start.2 = (bf16[1408,512]{1,0:T(8,128)(2,1)}, bf16[1408,512]{1,0:T(8,128)(2,1)}, u32[]{:S(2)}, u32[]{:S(2)}) collective-permute-start(bf16[1408,512]{1,0:T(8,128)(2,1)} %collective-permute-done.1), channel_id=1, source_target_pairs={{0,12},{4,0},{8,4},{12,8},{1,13},{5,1},{9,5},{13,9},{2,14},{6,2},{... | collective-permute-start | bytes 4325384 | tf_op jit(solution)/shard_map/ppermute | solution.py:14
  256.4 121.6 %copy-start.3 = (bf16[192,512]{1,0:T(8,128)(2,1)S(1)}, bf16[192,512]{1,0:T(8,128)(2,1)}, u32[]{:S(2)}) copy-start(bf16[192,512]{1,0:T(8,128)(2,1)} %reduce-scatter.3.cloned.1.call-done) | copy-start | bytes 589828
Sparse Core Ops, SparseCore 0:
  58.4 24.3 reduce-scatter.2
  356.4 21.4 reduce-scatter.4
Sparse Core Ops, SparseCore 1:
  60.3 162.1 all-gather.2
  223.9 124.5 all-gather.4
